TPU v7x, 32 devices: a whole 2x2x4 slice. The times are simulated.
32 devices in a mesh: ep: 8 (over z, y), tp: 4 (over x, core).
Axes of the slice: x: 2, y: 2, z: 4, core: 2. Of those that a mesh axis runs over, the one named last changes fastest.
Arguments:
- tokens: bfloat16 [6144, 2048], P('ep', 'tp')
- norm_gain: float32 [2048], P('tp'), may hold values from 0.1 to 1.9
- routing: int32 [6144, 2], P('ep'), may hold values from 0 to 7, as said below
- route_weight: float32 [6144, 2], P('ep'), may hold values from 0.2 to 1
- w_gate: bfloat16 [8, 2048, 512], P('ep', 'tp'), may hold values from -0.125 to 0.125
- w_up: bfloat16 [8, 2048, 512], P('ep', 'tp'), may hold values from -0.125 to 0.125
- w_down: bfloat16 [8, 512, 2048], P('ep', None, 'tp'), may hold values from -0.25 to 0.25
- w_branch_in: bfloat16 [2048, 1024], P('ep', 'tp'), may hold values from -0.125 to 0.125
- w_branch_out: bfloat16 [1024, 2048], P('tp', 'ep'), may hold values from -0.1875 to 0.1875
- branch_gate: float32 [2048], P('tp'), may hold values from -3 to 3
Outputs:
- mixed: bfloat16 [6144, 2048], P('ep', 'tp')
Inputs may be any that keep to these rules, and one draw needn't show every extreme that they name: `routing`: each row names two different experts of the same group; expert e belongs to group e // 2. Among the rows of one device (aligned blocks of 768 rows) no expert is named more than 384 times, and in every block all experts of one group are named exactly 384 times.
All inputs are finite; a program needn't handle non-finite values.
Results may differ from a plain program's by a relative error of at most 0.0069.
Values may be sent and summed in bfloat16 or wider, within the bound.
A program may use at most 128 MiB of HBM per device.

v0:
```python
import functools

import jax
import jax.numpy as jnp
from jax import lax
from jax.experimental import pallas as pl
from jax.experimental.pallas import tpu as pltpu
from jax.sharding import PartitionSpec as P

GROUPS = 4


epsilon = 1e-06


def send_back(result):
    return lax.all_to_all(result, "ep", split_axis=0, concat_axis=0, tiled=True)


def body(
    tokens,
    norm_gain,
    routing,
    route_weight,
    w_gate,
    w_up,
    w_down,
    w_branch_in,
    w_branch_out,
    branch_gate,
):
    token_count, quarter = tokens.shape
    full_width = quarter * lax.axis_size("tp")
    floats = tokens.astype(jnp.float32)
    squares = lax.psum(jnp.sum(floats * floats, axis=1), "tp")
    normed = (floats * lax.rsqrt(squares[:, None] / full_width + epsilon) * norm_gain).astype(
        jnp.bfloat16
    )
    expert_count = lax.axis_size("ep") * w_gate.shape[0]
    capacity = token_count // (expert_count // GROUPS)
    flat_ids = routing.reshape(-1)
    one_hot = (flat_ids[:, None] == jnp.arange(expert_count, dtype=jnp.int32)[None, :]).astype(
        jnp.int32
    )
    before = jnp.cumsum(one_hot, axis=0) - one_hot
    position = flat_ids * capacity + jnp.sum(before * one_hot, axis=1)
    copies = jnp.repeat(normed, 2, axis=0)
    buffer = jnp.zeros((expert_count * capacity, quarter), jnp.bfloat16).at[position].set(copies)
    buffer = buffer.reshape(expert_count, capacity, quarter)
    gate_whole, up_whole, down_whole = (
        lax.all_gather(w_gate[0], "tp", axis=0, tiled=True),
        lax.all_gather(w_up[0], "tp", axis=0, tiled=True),
        lax.all_gather(w_down[0], "tp", axis=1, tiled=True),
    )
    row_split = lax.all_to_all(
        lax.all_to_all(buffer, "ep", split_axis=0, concat_axis=0, tiled=True),
        "tp",
        split_axis=0,
        concat_axis=2,
        tiled=True,
    )
    slot_rows = row_split.reshape(-1, row_split.shape[2])
    gate_sum = jnp.dot(slot_rows, gate_whole, preferred_element_type=jnp.float32)
    up_sum = jnp.dot(slot_rows, up_whole, preferred_element_type=jnp.float32)
    hidden = (jax.nn.silu(gate_sum) * up_sum).astype(jnp.bfloat16)
    result = jnp.dot(hidden, down_whole, preferred_element_type=jnp.float32).astype(jnp.bfloat16)
    feature_split = lax.all_to_all(
        result.reshape(row_split.shape), "tp", split_axis=2, concat_axis=0, tiled=True
    )
    returned = send_back(feature_split)
    picked = returned.reshape(expert_count * capacity, quarter)[position].reshape(
        token_count, 2, quarter
    )
    routed = jnp.sum(picked.astype(jnp.float32) * route_weight[:, :, None], axis=1)
    branch_tokens = lax.all_to_all(normed, "tp", split_axis=0, concat_axis=1, tiled=True)
    in_cols, out_rows = (
        lax.all_gather(w_branch_in, "tp", axis=1, tiled=True),
        lax.all_gather(w_branch_out, "tp", axis=0, tiled=True),
    )
    in_whole, out_whole = (
        lax.all_gather(in_cols, "ep", axis=0, tiled=True),
        lax.all_gather(out_rows, "ep", axis=1, tiled=True),
    )
    branch_hidden = jax.nn.silu(
        jnp.dot(branch_tokens, in_whole, preferred_element_type=jnp.float32)
    ).astype(jnp.bfloat16)
    branch_local = jnp.dot(branch_hidden, out_whole, preferred_element_type=jnp.float32).astype(
        jnp.bfloat16
    )
    branch = lax.all_to_all(branch_local, "tp", split_axis=1, concat_axis=0, tiled=True)
    return (routed + jax.nn.sigmoid(branch_gate) * branch.astype(jnp.float32)).astype(jnp.bfloat16)


BF16, F32 = jnp.bfloat16, jnp.float32
COPIES = 53


def dot(a, b):
    return jnp.dot(a, b, preferred_element_type=F32)


def dot_nt(a, b):
    return lax.dot_general(a, b, (((1,), (1,)), ((), ())), preferred_element_type=F32)


def silu(v):
    return v / (1.0 + jnp.exp(-v))


def pair_kernel(
    tokens,
    gain,
    routing,
    route_weight,
    w_gate,
    w_up,
    w_down,
    w_in,
    w_out,
    branch_gate,
    out,
    gate_all,
    up_all,
    down_all,
    squares,
    normed,
    branch_all,
    slots_out,
    slots,
    slots_s,
    scale_out,
    scale,
    part_out,
    part_own,
    part_in,
    hidden,
    half_out,
    half_own,
    half_in,
    back_out,
    back,
    fold_out,
    fold_own,
    fold_in,
    cross_out,
    cross_in,
    branch_hidden,
    code_col,
    send_sem,
    recv_sem,
):
    ep, tp = lax.axis_index("ep"), lax.axis_index("tp")
    z, y, x, c = ep // 2, ep % 2, tp // 2, tp % 2
    token_count, quarter = tokens.shape
    ff = w_gate.shape[1]
    capacity = slots.shape[1]
    half = capacity // 2
    block = w_in.shape[0]

    def at(zz, yy, xx, cc):
        return (zz * 2 + yy, xx * 2 + cc)

    sibling = at(z, y, x, 1 - c)
    across = at(z, y, 1 - x, c)
    diagonal = at(z, y, 1 - x, 1 - c)
    pair = at(z, 1 - y, x, c)
    pair_user = at(z, 1 - y, x, y)
    pair_other = at(z, 1 - y, x, 1 - c)
    level = [z, z + 1 - 2 * (z % 2), (z + 2) % GROUPS, GROUPS - 1 - z]
    peer_of = [None] + [at(level[m], y, x, c) for m in range(1, GROUPS)]
    up = at((z + 1) % GROUPS, y, x, c)
    down = at((z + GROUPS - 1) % GROUPS, y, x, c)

    barrier = pltpu.get_barrier_semaphore()
    peers = [sibling, across, diagonal, pair, pair_other] + peer_of[1:]
    for peer in peers:
        pl.semaphore_signal(
            barrier, inc=1, device_id=peer, device_id_type=pl.DeviceIdType.MESH
        )

    branch_all[y, z, 0] = w_in[...]
    branch_all[y, z, 1] = w_out[...]
    floats = tokens[...].astype(F32)
    exact = floats * floats
    high = exact.astype(BF16)
    low = (exact - high.astype(F32)).astype(BF16)
    ones = jnp.ones((16, quarter), BF16)
    squares[0] = (dot_nt(ones, high) + dot_nt(ones, low))[:8]

    pl.semaphore_wait(barrier, len(peers))

    started = {}

    def send(number, source, target, device):
        copy = pltpu.make_async_remote_copy(
            src_ref=source,
            dst_ref=target,
            send_sem=send_sem.at[number],
            recv_sem=recv_sem.at[number],
            device_id=device,
            device_id_type=pl.DeviceIdType.MESH,
        )
        copy.start()
        started[number] = copy

    def arrived(number):
        started[number].wait_recv()

    send(6, squares.at[0], squares.at[1], sibling)
    send(7, squares.at[0], squares.at[2], across)
    send(8, squares.at[0], squares.at[3], diagonal)

    weights_of = ((w_gate, gate_all), (w_up, up_all), (w_down, down_all))

    def weight_copy(k, sem, device):
        source, target = weights_of[k]
        return pltpu.make_async_remote_copy(
            src_ref=source,
            dst_ref=target.at[c],
            send_sem=send_sem.at[2 * k + sem],
            recv_sem=recv_sem.at[2 * k + c],
            device_id=device,
            device_id_type=pl.DeviceIdType.MESH,
        )

    for k in range(3):
        weight_copy(k, 0, pair_user).start()

    @pl.when(c != y)
    def _():
        for k in range(3):
            weight_copy(k, 1, sibling).start()

    @pl.when(c == y)
    def _():
        for source, target in weights_of:
            target[c] = source[...]

    def weight_arrived(k):
        source, target = weights_of[k]

        def wait(h):
            pltpu.make_async_remote_copy(
                src_ref=source,
                dst_ref=target.at[h],
                send_sem=send_sem.at[2 * k],
                recv_sem=recv_sem.at[2 * k + h],
                device_id=sibling,
                device_id_type=pl.DeviceIdType.MESH,
            ).wait_recv()

        wait(1 - c)

        @pl.when(c != y)
        def _():
            wait(c)

    def relay(hop, upward):
        number = (12 if upward else 47) + hop - 1
        held = z - (hop - 1) if upward else z + (hop - 1)
        came = z - hop if upward else z + hop
        held, came = (held + GROUPS) % GROUPS, (came + GROUPS) % GROUPS
        sends = (z <= GROUPS - 2) & (z >= hop - 1)
        gets = z >= hop
        if not upward:
            sends = (z >= 1) & (z <= GROUPS - hop)
            gets = z <= GROUPS - 1 - hop

        def copy(row):
            return pltpu.make_async_remote_copy(
                src_ref=branch_all.at[y, row],
                dst_ref=branch_all.at[y, row],
                send_sem=send_sem.at[number],
                recv_sem=recv_sem.at[number],
                device_id=up if upward else down,
                device_id_type=pl.DeviceIdType.MESH,
            )

        return sends, gets, lambda: copy(held), lambda: copy(came)

    def relay_start(hop):
        for upward in (True, False):
            sends, _, outgoing, _ = relay(hop, upward)

            @pl.when(sends)
            def _():
                outgoing().start()

    def relay_arrived(hop):
        for upward in (True, False):
            _, gets, _, incoming = relay(hop, upward)

            @pl.when(gets)
            def _():
                incoming().wait_recv()

    def relay_sent(hop):
        for upward in (True, False):
            sends, _, outgoing, _ = relay(hop, upward)

            @pl.when(sends)
            def _():
                outgoing().wait_send()

    relay_start(1)
    ids = routing[0:1, :]
    group = lax.shift_right_logical(ids, 1)
    rows16 = lax.broadcasted_iota(jnp.int32, (16, token_count), 0)
    member = jnp.where(rows16 == group, 1.0, 0.0)
    earlier = jnp.where(
        lax.broadcasted_iota(jnp.int32, (token_count, token_count), 0)
        < lax.broadcasted_iota(jnp.int32, (token_count, token_count), 1),
        1.0,
        0.0,
    ).astype(BF16)
    before = dot(member.astype(BF16), earlier)
    place = jnp.sum(member * before, axis=0, keepdims=True)
    code = group.astype(F32) * capacity + place
    code_col[...] = jnp.transpose(jnp.broadcast_to(code, (8, token_count)))
    first, second = route_weight[0:1, :], route_weight[1:2, :]
    even_first = (ids & 1) == 0
    for_even = jnp.where(even_first, first, second)
    for_odd = jnp.where(even_first, second, first)
    weights = jnp.where((rows16 & 1) == 0, for_even, for_odd)
    weights_high = weights.astype(BF16)
    weights_low = (weights - weights_high.astype(F32)).astype(BF16)

    for number in (6, 7, 8):
        arrived(number)
    total = squares[0] + squares[1] + squares[2] + squares[3]
    factor = lax.rsqrt(total / (4 * quarter) + epsilon)
    factor_col = jnp.transpose(factor)[:, 0:1]
    normed[0] = (tokens[...].astype(F32) * factor_col * gain[...]).astype(BF16)
    send(10, normed.at[0], normed.at[2], across)
    send(9, normed.at[0], normed.at[1], sibling)

    def dispatch(s):
        send(19 + s, slots_out.at[s], slots.at[s], peer_of[s])
        send(22 + s, scale_out.at[s], scale.at[s], peer_of[s])

    slot_row = lax.broadcasted_iota(jnp.int32, (capacity, token_count), 0)
    for s in (2, 3, 1, 0):
        wanted = (slot_row + level[s] * capacity).astype(F32)
        choose = jnp.where(wanted == code, 1.0, 0.0).astype(BF16)
        rows = dot(choose, normed[0]).astype(BF16)
        slot_weights = (dot_nt(weights_high, choose) + dot_nt(weights_low, choose))[:8]
        if s == 0:
            slots[0] = rows
            scale[0] = slot_weights
            send(26, slots.at[0], slots_s.at[0], sibling)
        else:
            slots_out[s] = rows
            scale_out[s] = slot_weights
            if s > 1:
                dispatch(s)

    def project(s, start, weights):
        own = slots[s, pl.ds(start, half), :]
        other = slots_s[s, pl.ds(start, half), :]
        return dot(own, weights[c]) + dot(other, weights[1 - c])

    mine = pl.multiple_of(x * half, half)
    theirs = pl.multiple_of((1 - x) * half, half)

    def forward(s):
        if s:
            arrived(19 + s)
            send(26 + s, slots.at[s], slots_s.at[s], sibling)

    sides = (slice(0, ff), slice(ff, 2 * ff))

    def stage_a(s):
        arrived(26 + s)
        for side, weights in zip(sides, (gate_all, up_all)):
            part_out[s, :, side] = project(s, theirs, weights).astype(BF16)
        send(30 + s, part_out.at[s], part_in.at[s], across)
        for side, weights in zip(sides, (gate_all, up_all)):
            part_own[s, :, side] = project(s, mine, weights)

    def stage_a_own(k):
        side, weights = sides[k], (gate_all, up_all)[k]
        part_out[0, :, side] = project(0, theirs, weights).astype(BF16)
        send(30 + 20 * k, part_out.at[0, :, side], part_in.at[0, :, side], across)
        part_own[0, :, side] = project(0, mine, weights)

    def stage_b(s):
        arrived(30 + s)
        if s == 0:
            arrived(50)
        gate_sum = part_own[s, :, :ff] + part_in[s, :, :ff].astype(F32)
        up_sum = part_own[s, :, ff:] + part_in[s, :, ff:].astype(F32)
        hidden[s, pl.ds(mine, half), :] = (silu(gate_sum) * up_sum).astype(BF16)
        kept = hidden.at[s, pl.ds(mine, half), :]
        send(34 + s, kept, kept, across)

    def stage_c(s):
        arrived(34 + s)
        if s:
            arrived(22 + s)
        columns = jnp.transpose(scale[s])
        weight = jnp.where(c == 0, columns[:, 0:1], columns[:, 1:2])
        units = hidden[s]
        half_out[s] = (dot(units, down_all[1 - c]) * weight).astype(BF16)
        send(38 + s, half_out.at[s], half_in.at[s], sibling)
        half_own[s] = dot(units, down_all[c]) * weight

    def stage_d(s):
        arrived(38 + s)
        both = (half_own[s] + half_in[s].astype(F32)).astype(BF16)
        if s == 0:
            back[0] = both
        else:
            back_out[s] = both
            send(41 + s, back_out.at[s], back.at[s], peer_of[s])

    def pair_send(m):
        rows = branch_all.at[y, level[m]]
        send(15 + m, rows, rows, pair)

    weight_arrived(0)
    arrived(26)
    stage_a_own(0)
    weight_arrived(1)
    stage_a_own(1)
    dispatch(1)
    relay_arrived(1)
    relay_start(2)
    pair_send(0)
    pair_send(1)
    forward(2)
    stage_a(2)
    arrived(10)
    send(11, normed.at[2], normed.at[3], sibling)
    stage_b(0)
    forward(3)
    stage_a(3)
    relay_arrived(2)
    relay_start(3)
    pair_send(2)
    stage_b(2)
    stage_b(3)
    relay_arrived(3)
    pair_send(3)
    weight_arrived(2)
    stage_c(2)
    forward(1)
    stage_a(1)
    stage_d(2)
    stage_c(3)
    stage_c(0)
    stage_d(3)
    stage_d(0)

    arrived(9)
    arrived(11)
    for m in range(GROUPS):
        arrived(15 + m)
    quarters = (tp, x * 2 + 1 - c, (1 - x) * 2 + c, (1 - x) * 2 + 1 - c)
    sums = jnp.zeros((token_count, block), F32)
    for k, q in enumerate(quarters):
        sums = sums + dot(normed[k, :, :block], branch_all[0, q, 0])
        sums = sums + dot(normed[k, :, block:], branch_all[1, q, 0])
    branch_hidden[...] = silu(sums).astype(BF16)

    def branch_part(q, side):
        return dot(branch_hidden[...], branch_all[side, q, 1])

    for side in range(2):
        columns = slice(side * block, (side + 1) * block)
        fold_out[0, :, columns] = branch_part(quarters[1], side).astype(BF16)
        fold_out[1, :, columns] = branch_part(quarters[3], side).astype(BF16)
    send(45, fold_out, fold_in, sibling)

    stage_b(1)

    arrived(45)
    for side in range(2):
        columns = slice(side * block, (side + 1) * block)
        cross_out[:, columns] = (
            branch_part(quarters[2], side) + fold_in[1, :, columns].astype(F32)
        ).astype(BF16)
    send(46, cross_out, cross_in, across)
    stage_c(1)
    stage_d(1)
    for side in range(2):
        columns = slice(side * block, (side + 1) * block)
        fold_own[:, columns] = branch_part(quarters[0], side) + fold_in[0, :, columns].astype(F32)

    slot_lane = lax.broadcasted_iota(jnp.int32, (token_count, capacity), 1)

    def restore(s):
        wanted = (slot_lane + level[s] * capacity).astype(F32)
        choose = jnp.where(wanted == code_col[:, 0:1], 1.0, 0.0).astype(BF16)
        return dot(choose, back[s])

    half_own_sum = restore(0)
    for s in (2, 3, 1):
        arrived(41 + s)
        half_own_sum = half_own_sum + restore(s)
    arrived(46)
    branch = fold_own[...] + cross_in[...].astype(F32)
    gate = 1.0 / (1.0 + jnp.exp(-branch_gate[...]))
    out[...] = (half_own_sum + gate * branch).astype(BF16)
    for copy in started.values():
        copy.wait_send()
    for hop in range(1, GROUPS):
        relay_sent(hop)
    for k in range(3):
        weight_copy(k, 0, pair_user).wait_send()

    @pl.when(c != y)
    def _():
        for k in range(3):
            weight_copy(k, 1, sibling).wait_send()


def pair_body(
    tokens,
    norm_gain,
    routing,
    route_weight,
    w_gate,
    w_up,
    w_down,
    w_branch_in,
    w_branch_out,
    branch_gate,
):
    count, quarter = tokens.shape
    ff = w_gate.shape[2]
    block = w_branch_in.shape[0]
    cap = count // 2
    half = cap // 2
    vmem = pltpu.VMEM
    rows = (GROUPS, cap, quarter)
    scratch = [
        vmem((2, quarter, ff), BF16),
        vmem((2, quarter, ff), BF16),
        vmem((2, ff, quarter), BF16),
        vmem((4, 8, count), F32),
        vmem((4, count, quarter), BF16),
        vmem((2, GROUPS, 2, block, block), BF16),
        vmem(rows, BF16),
        vmem(rows, BF16),
        vmem(rows, BF16),
        vmem((GROUPS, 8, cap), F32),
        vmem((GROUPS, 8, cap), F32),
        vmem((GROUPS, half, 2 * ff), BF16),
        vmem((GROUPS, half, 2 * ff), F32),
        vmem((GROUPS, half, 2 * ff), BF16),
        vmem((GROUPS, cap, ff), BF16),
        vmem(rows, BF16),
        vmem(rows, F32),
        vmem(rows, BF16),
        vmem(rows, BF16),
        vmem(rows, BF16),
        vmem((2, count, quarter), BF16),
        vmem((count, quarter), F32),
        vmem((2, count, quarter), BF16),
        vmem((count, quarter), BF16),
        vmem((count, quarter), BF16),
        vmem((count, block), BF16),
        vmem((count, 8), F32),
        pltpu.SemaphoreType.DMA((COPIES,)),
        pltpu.SemaphoreType.DMA((COPIES,)),
    ]
    return pl.pallas_call(
        pair_kernel,
        out_shape=jax.ShapeDtypeStruct((count, quarter), BF16),
        in_specs=[pl.BlockSpec(memory_space=vmem)] * 10,
        out_specs=pl.BlockSpec(memory_space=vmem),
        scratch_shapes=scratch,
        compiler_params=pltpu.CompilerParams(
            collective_id=0, has_side_effects=True, vmem_limit_bytes=60 * 1024 * 1024
        ),
    )(
        tokens,
        norm_gain[None, :],
        routing.T,
        route_weight.T,
        w_gate[0],
        w_up[0],
        w_down[0],
        w_branch_in,
        w_branch_out,
        branch_gate[None, :],
    )


def solution(mesh):
    return jax.shard_map(
        pair_body if mesh.shape["ep"] == 2 * GROUPS and mesh.shape["tp"] == 4 else body,
        mesh=mesh,
        in_specs=(
            P("ep", "tp"),
            P("tp"),
            P("ep", None),
            P("ep", None),
            P("ep", "tp", None),
            P("ep", "tp", None),
            P("ep", None, "tp"),
            P("ep", "tp"),
            P("tp", "ep"),
            P("tp"),
        ),
        out_specs=P("ep", "tp"),
        check_vma=False,
    )
```

profile of v0, /device:TPU:0, one launch (start us, length us, event | category | flops | bytes accessed | tf_op | source)
XLA Modules:
  0.0 109.4 jit_solution(3779288972032764048)
XLA Ops:
  0.0 107.3 %shard_map.100 = bf16[768,512]{1,0:T(8,128)(2,1)} custom-call(bf16[768,512]{1,0:T(8,128)(2,1)} %tokens.1, f32[1,512]{1,0:T(1,128)} %bitcast.12, s32[2,768]{1,0:T(2,128)} %bitcast.10, f32[2,768]{1,0:T(2,128)} %bitcast.11, bf16[512,512]{1,0:T(8,128)(2,1)} %bitcast.7, bf16[512,512]{1,0:T(8,128)(2,1)} %bitcast.8, bf16[512,512]{1,0:T(8,128)(2,1)} %bitcast.9, ...), custom_call_target="tpu_custom_call" | custom-call | tf_op jit(solution)/shard_map/pallas_call | solution.py:567
  107.3 2.1 %copy.12 = bf16[768,512]{1,0:T(8,128)(2,1)} copy(bf16[768,512]{1,0:T(8,128)(2,1)} %shard_map.100) | data formatting | bytes 1572864
where the time goes:
time: 110 us; the launch traced here: 109 us
  Pallas kernels  107 us (97%)
  local copies, waits for them, and re-layouts  2.06 us (2%)
    pallas_call x1, Pallas kernels, pair_body(): pl.pallas_call(pair_kernel, out_shape=jax.ShapeDtypeStruct((count, quarte...  107 us

commit v1 on v0

v1 whole, which is shorter than its diff:
```python
import functools

import jax
import jax.numpy as jnp
from jax import lax
from jax.experimental import pallas as pl
from jax.experimental.pallas import tpu as pltpu
from jax.sharding import PartitionSpec as P

GROUPS = 4


epsilon = 1e-06


def send_back(result):
    return lax.all_to_all(result, "ep", split_axis=0, concat_axis=0, tiled=True)


def body(
    tokens,
    norm_gain,
    routing,
    route_weight,
    w_gate,
    w_up,
    w_down,
    w_branch_in,
    w_branch_out,
    branch_gate,
):
    token_count, quarter = tokens.shape
    full_width = quarter * lax.axis_size("tp")
    floats = tokens.astype(jnp.float32)
    squares = lax.psum(jnp.sum(floats * floats, axis=1), "tp")
    normed = (floats * lax.rsqrt(squares[:, None] / full_width + epsilon) * norm_gain).astype(
        jnp.bfloat16
    )
    expert_count = lax.axis_size("ep") * w_gate.shape[0]
    capacity = token_count // (expert_count // GROUPS)
    flat_ids = routing.reshape(-1)
    one_hot = (flat_ids[:, None] == jnp.arange(expert_count, dtype=jnp.int32)[None, :]).astype(
        jnp.int32
    )
    before = jnp.cumsum(one_hot, axis=0) - one_hot
    position = flat_ids * capacity + jnp.sum(before * one_hot, axis=1)
    copies = jnp.repeat(normed, 2, axis=0)
    buffer = jnp.zeros((expert_count * capacity, quarter), jnp.bfloat16).at[position].set(copies)
    buffer = buffer.reshape(expert_count, capacity, quarter)
    gate_whole, up_whole, down_whole = (
        lax.all_gather(w_gate[0], "tp", axis=0, tiled=True),
        lax.all_gather(w_up[0], "tp", axis=0, tiled=True),
        lax.all_gather(w_down[0], "tp", axis=1, tiled=True),
    )
    row_split = lax.all_to_all(
        lax.all_to_all(buffer, "ep", split_axis=0, concat_axis=0, tiled=True),
        "tp",
        split_axis=0,
        concat_axis=2,
        tiled=True,
    )
    slot_rows = row_split.reshape(-1, row_split.shape[2])
    gate_sum = jnp.dot(slot_rows, gate_whole, preferred_element_type=jnp.float32)
    up_sum = jnp.dot(slot_rows, up_whole, preferred_element_type=jnp.float32)
    hidden = (jax.nn.silu(gate_sum) * up_sum).astype(jnp.bfloat16)
    result = jnp.dot(hidden, down_whole, preferred_element_type=jnp.float32).astype(jnp.bfloat16)
    feature_split = lax.all_to_all(
        result.reshape(row_split.shape), "tp", split_axis=2, concat_axis=0, tiled=True
    )
    returned = send_back(feature_split)
    picked = returned.reshape(expert_count * capacity, quarter)[position].reshape(
        token_count, 2, quarter
    )
    routed = jnp.sum(picked.astype(jnp.float32) * route_weight[:, :, None], axis=1)
    branch_tokens = lax.all_to_all(normed, "tp", split_axis=0, concat_axis=1, tiled=True)
    in_cols, out_rows = (
        lax.all_gather(w_branch_in, "tp", axis=1, tiled=True),
        lax.all_gather(w_branch_out, "tp", axis=0, tiled=True),
    )
    in_whole, out_whole = (
        lax.all_gather(in_cols, "ep", axis=0, tiled=True),
        lax.all_gather(out_rows, "ep", axis=1, tiled=True),
    )
    branch_hidden = jax.nn.silu(
        jnp.dot(branch_tokens, in_whole, preferred_element_type=jnp.float32)
    ).astype(jnp.bfloat16)
    branch_local = jnp.dot(branch_hidden, out_whole, preferred_element_type=jnp.float32).astype(
        jnp.bfloat16
    )
    branch = lax.all_to_all(branch_local, "tp", split_axis=1, concat_axis=0, tiled=True)
    return (routed + jax.nn.sigmoid(branch_gate) * branch.astype(jnp.float32)).astype(jnp.bfloat16)


BF16, F32 = jnp.bfloat16, jnp.float32
COPIES = 54
VMEM_LIMIT = 46 * 1024 * 1024


def dot(a, b):
    return jnp.dot(a, b, preferred_element_type=F32)


def dot_nt(a, b):
    return lax.dot_general(a, b, (((1,), (1,)), ((), ())), preferred_element_type=F32)


def silu(v):
    return v / (1.0 + jnp.exp(-v))


def pair_kernel(
    tokens_hbm,
    gain_hbm,
    routing_hbm,
    route_weight_hbm,
    w_gate,
    w_up,
    w_down,
    w_in,
    w_out,
    branch_gate_hbm,
    out,
    tokens,
    gain,
    routing,
    route_weight,
    branch_gate,
    gate_all,
    up_all,
    down_all,
    squares,
    scaled,
    branch_all,
    chosen,
    slots_out,
    slots,
    slots_s,
    scale_out,
    scale,
    scale_col,
    part_out,
    part_own,
    part_in,
    hidden,
    half_out,
    half_own,
    half_in,
    back_out,
    back,
    fold_out,
    fold_own,
    fold_in,
    cross_out,
    cross_in,
    branch_hidden,
    code_col,
    factor_col,
    load_sem,
    send_sem,
    recv_sem,
):
    ep, tp = lax.axis_index("ep"), lax.axis_index("tp")
    z, y, x, c = ep // 2, ep % 2, tp // 2, tp % 2
    token_count, quarter = tokens.shape
    ff = w_gate.shape[1]
    capacity = slots.shape[1]
    half = capacity // 2
    block = w_in.shape[0]

    def at(zz, yy, xx, cc):
        return (zz * 2 + yy, xx * 2 + cc)

    sibling = at(z, y, x, 1 - c)
    across = at(z, y, 1 - x, c)
    diagonal = at(z, y, 1 - x, 1 - c)
    pair = at(z, 1 - y, x, c)
    pair_user = at(z, 1 - y, x, y)
    pair_other = at(z, 1 - y, x, 1 - c)
    level = [z, z + 1 - 2 * (z % 2), (z + 2) % GROUPS, GROUPS - 1 - z]
    peer_of = [None] + [at(level[m], y, x, c) for m in range(1, GROUPS)]
    up = at((z + 1) % GROUPS, y, x, c)
    down = at((z + GROUPS - 1) % GROUPS, y, x, c)

    barrier = pltpu.get_barrier_semaphore()
    peers = [sibling, across, diagonal, pair, pair_other] + peer_of[1:]
    for peer in peers:
        pl.semaphore_signal(
            barrier, inc=1, device_id=peer, device_id_type=pl.DeviceIdType.MESH
        )

    loads = [
        pltpu.make_async_copy(source, target, load_sem.at[number])
        for number, (source, target) in enumerate(
            (
                (routing_hbm, routing),
                (tokens_hbm, tokens),
                (gain_hbm, gain),
                (route_weight_hbm, route_weight),
                (branch_gate_hbm, branch_gate),
                (w_in, branch_all.at[y, z, 0]),
                (w_out, branch_all.at[y, z, 1]),
            )
        )
    ]
    for load in loads:
        load.start()

    weights_of = ((w_gate, gate_all), (w_up, up_all), (w_down, down_all))

    def weight_load(k):
        source, target = weights_of[k]
        return pltpu.make_async_copy(source, target.at[c], load_sem.at[len(loads) + k])

    @pl.when(c == y)
    def _():
        for k in range(3):
            weight_load(k).start()

    loads[0].wait()
    ids = routing[0:1, :]
    group = lax.shift_right_logical(ids, 1)
    rows16 = lax.broadcasted_iota(jnp.int32, (16, token_count), 0)
    member = jnp.where(rows16 == group, 1.0, 0.0)
    earlier = jnp.where(
        lax.broadcasted_iota(jnp.int32, (token_count, token_count), 0)
        < lax.broadcasted_iota(jnp.int32, (token_count, token_count), 1),
        1.0,
        0.0,
    ).astype(BF16)
    before = dot(member.astype(BF16), earlier)
    place = jnp.sum(member * before, axis=0, keepdims=True)
    code = group.astype(F32) * capacity + place

    loads[1].wait()
    loads[2].wait()
    floats = tokens[...].astype(F32)
    scaled[0] = (floats * gain[...]).astype(BF16)
    exact = floats * floats
    high = exact.astype(BF16)
    low = (exact - high.astype(F32)).astype(BF16)
    ones = jnp.ones((16, quarter), BF16)
    squares[0] = (dot_nt(ones, high) + dot_nt(ones, low))[:8]

    slot_row = lax.broadcasted_iota(jnp.int32, (capacity, token_count), 0)

    def choose_rows(s):
        wanted = (slot_row + level[s] * capacity).astype(F32)
        chosen[s] = jnp.where(wanted == code, 1.0, 0.0).astype(BF16)
        rows = dot(chosen[s], scaled[0]).astype(BF16)
        if s == 0:
            slots[0] = rows
        else:
            slots_out[s] = rows

    choose_rows(2)

    pl.semaphore_wait(barrier, len(peers))

    started = {}

    def send(number, source, target, device):
        copy = pltpu.make_async_remote_copy(
            src_ref=source,
            dst_ref=target,
            send_sem=send_sem.at[number],
            recv_sem=recv_sem.at[number],
            device_id=device,
            device_id_type=pl.DeviceIdType.MESH,
        )
        copy.start()
        started[number] = copy

    def send_if(condition, number, source, target, device):
        copy = pltpu.make_async_remote_copy(
            src_ref=source,
            dst_ref=target,
            send_sem=send_sem.at[number],
            recv_sem=recv_sem.at[number],
            device_id=device,
            device_id_type=pl.DeviceIdType.MESH,
        )

        @pl.when(condition)
        def _():
            copy.start()

        started[number] = copy

    def arrived(number):
        started[number].wait_recv()

    def weight_copy(k, sem, device):
        source, target = weights_of[k]
        return pltpu.make_async_remote_copy(
            src_ref=source,
            dst_ref=target.at[c],
            send_sem=send_sem.at[2 * k + sem],
            recv_sem=recv_sem.at[2 * k + c],
            device_id=device,
            device_id_type=pl.DeviceIdType.MESH,
        )

    def send_slots(s):
        send(19 + s, slots_out.at[s], slots.at[s], peer_of[s])

    def send_slots_if(condition, s):
        send_if(condition, 19 + s, slots_out.at[s], slots.at[s], peer_of[s])

    def send_scale(s):
        send(22 + s, scale_out.at[s], scale.at[s], peer_of[s])

    def relay(hop, upward):
        number = (12 if upward else 47) + hop - 1
        held = z - (hop - 1) if upward else z + (hop - 1)
        came = z - hop if upward else z + hop
        held, came = (held + GROUPS) % GROUPS, (came + GROUPS) % GROUPS
        sends = (z <= GROUPS - 2) & (z >= hop - 1)
        gets = z >= hop
        if not upward:
            sends = (z >= 1) & (z <= GROUPS - hop)
            gets = z <= GROUPS - 1 - hop

        def copy(row):
            return pltpu.make_async_remote_copy(
                src_ref=branch_all.at[y, row],
                dst_ref=branch_all.at[y, row],
                send_sem=send_sem.at[number],
                recv_sem=recv_sem.at[number],
                device_id=up if upward else down,
                device_id_type=pl.DeviceIdType.MESH,
            )

        return sends, gets, lambda: copy(held), lambda: copy(came)

    def relay_start(hop):
        for upward in (True, False):
            sends, _, outgoing, _ = relay(hop, upward)

            @pl.when(sends)
            def _():
                outgoing().start()

    def relay_arrived(hop):
        for upward in (True, False):
            _, gets, _, incoming = relay(hop, upward)

            @pl.when(gets)
            def _():
                incoming().wait_recv()

    def relay_sent(hop):
        for upward in (True, False):
            sends, _, outgoing, _ = relay(hop, upward)

            @pl.when(sends)
            def _():
                outgoing().wait_send()

    send(7, squares.at[0], squares.at[2], across)
    send(8, squares.at[0], squares.at[3], diagonal)
    send(6, squares.at[0], squares.at[1], sibling)
    outer = (z == 0) | (z == GROUPS - 1)
    early = c == y
    send_slots(2)
    loads[5].wait()
    loads[6].wait()
    relay_start(1)
    send_if(c != y, 10, scaled.at[0], scaled.at[2], across)
    for k in range(3):
        weight_copy(k, 0, pair_user).start()

    @pl.when(c != y)
    def _():
        for k in range(3):
            weight_copy(k, 1, sibling).start()

    send(9, scaled.at[0], scaled.at[1], sibling)

    def weight_arrived(k):
        source, target = weights_of[k]

        def wait(h):
            pltpu.make_async_remote_copy(
                src_ref=source,
                dst_ref=target.at[h],
                send_sem=send_sem.at[2 * k],
                recv_sem=recv_sem.at[2 * k + h],
                device_id=sibling,
                device_id_type=pl.DeviceIdType.MESH,
            ).wait_recv()

        wait(1 - c)

        @pl.when(c != y)
        def _():
            wait(c)

        @pl.when(c == y)
        def _():
            weight_load(k).wait()

    def pair_send(m):
        rows = branch_all.at[y, level[m]]
        send(15 + m, rows, rows, pair)

    choose_rows(0)
    send(26, slots.at[0], slots_s.at[0], sibling)
    choose_rows(1)
    choose_rows(3)
    pair_send(0)

    loads[3].wait()
    loads[4].wait()
    first, second = route_weight[0:1, :], route_weight[1:2, :]
    even_first = (ids & 1) == 0
    for_even = jnp.where(even_first, first, second)
    for_odd = jnp.where(even_first, second, first)
    for number in (6, 7, 8):
        arrived(number)
    total = squares[0] + squares[1] + squares[2] + squares[3]
    factor = lax.rsqrt(total / (4 * quarter) + epsilon)
    factor_col[...] = jnp.transpose(factor)
    code_col[...] = jnp.transpose(jnp.broadcast_to(code, (8, token_count)))
    weights = jnp.where(
        rows16 == 0, for_even, jnp.where(rows16 == 1, for_odd, factor[0:1, :])
    )
    weights_high = weights.astype(BF16)
    weights_low = (weights - weights_high.astype(F32)).astype(BF16)
    for s in (2, 1, 3, 0):
        slot_weights = (dot_nt(weights_high, chosen[s]) + dot_nt(weights_low, chosen[s]))[:8]
        if s == 0:
            scale[0] = slot_weights
        else:
            scale_out[s] = slot_weights
            send_scale(s)
    send_slots_if(outer, 1)
    send_slots_if(outer, 3)

    def project(s, start, weights):
        own = slots[s, pl.ds(start, half), :]
        other = slots_s[s, pl.ds(start, half), :]
        return dot(own, weights[c]) + dot(other, weights[1 - c])

    mine = pl.multiple_of(x * half, half)
    theirs = pl.multiple_of((1 - x) * half, half)

    def forward(s):
        if s:
            arrived(19 + s)
            send(26 + s, slots.at[s], slots_s.at[s], sibling)

    sides = (slice(0, ff), slice(ff, 2 * ff))

    def stage_a(s):
        arrived(26 + s)
        for side, weights in zip(sides, (gate_all, up_all)):
            part_out[s, :, side] = project(s, theirs, weights).astype(BF16)
        send(30 + s, part_out.at[s], part_in.at[s], across)
        for side, weights in zip(sides, (gate_all, up_all)):
            part_own[s, :, side] = project(s, mine, weights)

    def stage_a_side(s, k):
        if k == 0:
            arrived(26 + s)
        side, weights = sides[k], (gate_all, up_all)[k]
        part_out[s, :, side] = project(s, theirs, weights).astype(BF16)
        number = 30 + s if k == 0 else 50 + s
        send(number, part_out.at[s, :, side], part_in.at[s, :, side], across)
        part_own[s, :, side] = project(s, mine, weights)

    def stage_b(s):
        if s:
            arrived(22 + s)
        scale_col[s] = jnp.transpose(scale[s])
        arrived(30 + s)
        if 50 + s in started:
            arrived(50 + s)
        rescale = scale_col[s, pl.ds(mine, half), 2:3]
        gate_sum = (part_own[s, :, :ff] + part_in[s, :, :ff].astype(F32)) * rescale
        up_sum = (part_own[s, :, ff:] + part_in[s, :, ff:].astype(F32)) * rescale
        hidden[s, pl.ds(mine, half), :] = (silu(gate_sum) * up_sum).astype(BF16)
        kept = hidden.at[s, pl.ds(mine, half), :]
        send(34 + s, kept, kept, across)

    def stage_c(s):
        arrived(34 + s)
        weight = jnp.where(c == 0, scale_col[s, :, 0:1], scale_col[s, :, 1:2])
        units = hidden[s]
        half_out[s] = (dot(units, down_all[1 - c]) * weight).astype(BF16)
        send(38 + s, half_out.at[s], half_in.at[s], sibling)
        half_own[s] = dot(units, down_all[c]) * weight

    def stage_d(s):
        arrived(38 + s)
        both = (half_own[s] + half_in[s].astype(F32)).astype(BF16)
        if s == 0:
            back[0] = both
        else:
            back_out[s] = both
            send(41 + s, back_out.at[s], back.at[s], peer_of[s])

    quarters = (tp, x * 2 + 1 - c, (1 - x) * 2 + c, (1 - x) * 2 + 1 - c)

    def branch_first():
        sums = jnp.zeros((token_count, block), F32)
        for k, q in enumerate(quarters):
            sums = sums + dot(scaled[k, :, :block], branch_all[0, q, 0])
            sums = sums + dot(scaled[k, :, block:], branch_all[1, q, 0])
        branch_hidden[...] = silu(sums * factor_col[:, 0:1]).astype(BF16)

    def branch_part(q, side):
        return dot(branch_hidden[...], branch_all[side, q, 1])

    def branch_fold():
        for side in range(2):
            columns = slice(side * block, (side + 1) * block)
            fold_out[0, :, columns] = branch_part(quarters[1], side).astype(BF16)
            fold_out[1, :, columns] = branch_part(quarters[3], side).astype(BF16)
        send(45, fold_out, fold_in, sibling)

    def branch_cross():
        arrived(45)
        for side in range(2):
            columns = slice(side * block, (side + 1) * block)
            cross_out[:, columns] = (
                branch_part(quarters[2], side) + fold_in[1, :, columns].astype(F32)
            ).astype(BF16)
        send(46, cross_out, cross_in, across)

    def branch_own():
        for side in range(2):
            columns = slice(side * block, (side + 1) * block)
            fold_own[:, columns] = branch_part(quarters[0], side) + fold_in[
                0, :, columns
            ].astype(F32)

    slot_lane = lax.broadcasted_iota(jnp.int32, (token_count, capacity), 1)

    def restore(s):
        if s:
            arrived(41 + s)
        wanted = (slot_lane + level[s] * capacity).astype(F32)
        choose = jnp.where(wanted == code_col[:, 0:1], 1.0, 0.0).astype(BF16)
        return dot(choose, back[s])

    weight_arrived(0)
    stage_a_side(0, 0)
    weight_arrived(1)
    stage_a_side(0, 1)
    send_if(early, 10, scaled.at[0], scaled.at[2], across)
    forward(2)
    send_slots_if(~outer, 3)
    send_slots_if(~outer, 1)
    stage_a(2)
    stage_b(0)
    relay_arrived(1)
    relay_start(2)
    pair_send(1)
    arrived(10)
    send(11, scaled.at[2], scaled.at[3], sibling)
    forward(1)
    stage_b(2)
    weight_arrived(2)
    stage_c(0)
    stage_d(0)
    forward(3)
    stage_a(3)
    stage_c(2)
    stage_d(2)
    relay_arrived(2)
    relay_start(3)
    pair_send(2)
    stage_a_side(1, 0)
    stage_b(3)
    stage_a_side(1, 1)
    relay_arrived(3)
    pair_send(3)
    stage_c(3)
    stage_d(3)
    arrived(9)
    arrived(11)
    for m in range(GROUPS):
        arrived(15 + m)
    branch_first()
    branch_fold()
    stage_b(1)
    branch_cross()
    branch_own()
    stage_c(1)
    stage_d(1)

    half_own_sum = restore(0)
    for s in (2, 3, 1):
        half_own_sum = half_own_sum + restore(s)
    arrived(46)
    branch = fold_own[...] + cross_in[...].astype(F32)
    gate = 1.0 / (1.0 + jnp.exp(-branch_gate[...]))
    out[...] = (half_own_sum + gate * branch).astype(BF16)
    for copy in started.values():
        copy.wait_send()
    for hop in range(1, GROUPS):
        relay_sent(hop)
    for k in range(3):
        weight_copy(k, 0, pair_user).wait_send()

    @pl.when(c != y)
    def _():
        for k in range(3):
            weight_copy(k, 1, sibling).wait_send()


def pair_body(
    tokens,
    norm_gain,
    routing,
    route_weight,
    w_gate,
    w_up,
    w_down,
    w_branch_in,
    w_branch_out,
    branch_gate,
):
    count, quarter = tokens.shape
    ff = w_gate.shape[2]
    block = w_branch_in.shape[0]
    cap = count // 2
    half = cap // 2
    vmem = pltpu.VMEM
    rows = (GROUPS, cap, quarter)
    scratch = [
        vmem((count, quarter), BF16),
        vmem((1, quarter), F32),
        vmem((2, count), jnp.int32),
        vmem((2, count), F32),
        vmem((1, quarter), F32),
        vmem((2, quarter, ff), BF16),
        vmem((2, quarter, ff), BF16),
        vmem((2, ff, quarter), BF16),
        vmem((4, 8, count), F32),
        vmem((4, count, quarter), BF16),
        vmem((2, GROUPS, 2, block, block), BF16),
        vmem((GROUPS, cap, count), BF16),
        vmem(rows, BF16),
        vmem(rows, BF16),
        vmem(rows, BF16),
        vmem((GROUPS, 8, cap), F32),
        vmem((GROUPS, 8, cap), F32),
        vmem((GROUPS, cap, 8), F32),
        vmem((GROUPS, half, 2 * ff), BF16),
        vmem((GROUPS, half, 2 * ff), F32),
        vmem((GROUPS, half, 2 * ff), BF16),
        vmem((GROUPS, cap, ff), BF16),
        vmem(rows, BF16),
        vmem(rows, F32),
        vmem(rows, BF16),
        vmem(rows, BF16),
        vmem(rows, BF16),
        vmem((2, count, quarter), BF16),
        vmem((count, quarter), F32),
        vmem((2, count, quarter), BF16),
        vmem((count, quarter), BF16),
        vmem((count, quarter), BF16),
        vmem((count, block), BF16),
        vmem((count, 8), F32),
        vmem((count, 8), F32),
        pltpu.SemaphoreType.DMA((10,)),
        pltpu.SemaphoreType.DMA((COPIES,)),
        pltpu.SemaphoreType.DMA((COPIES,)),
    ]
    return pl.pallas_call(
        pair_kernel,
        out_shape=pltpu.VMEM((count, quarter), BF16),
        in_specs=[pl.BlockSpec(memory_space=pltpu.HBM)] * 10,
        out_specs=pl.BlockSpec(memory_space=vmem),
        scratch_shapes=scratch,
        compiler_params=pltpu.CompilerParams(
            collective_id=0, has_side_effects=True, vmem_limit_bytes=VMEM_LIMIT
        ),
    )(
        *(
            pltpu.with_memory_space_constraint(operand, pltpu.HBM)
            for operand in (
                tokens,
                norm_gain[None, :],
                routing.T,
                route_weight.T,
                w_gate[0],
                w_up[0],
                w_down[0],
                w_branch_in,
                w_branch_out,
                branch_gate[None, :],
            )
        )
    )


def solution(mesh):
    return jax.shard_map(
        pair_body if mesh.shape["ep"] == 2 * GROUPS and mesh.shape["tp"] == 4 else body,
        mesh=mesh,
        in_specs=(
            P("ep", "tp"),
            P("tp"),
            P("ep", None),
            P("ep", None),
            P("ep", "tp", None),
            P("ep", "tp", None),
            P("ep", None, "tp"),
            P("ep", "tp"),
            P("tp", "ep"),
            P("tp"),
        ),
        out_specs=P("ep", "tp"),
        check_vma=False,
    )
```

time: 110 us -> 101 us (0.918)
  Pallas kernels: 107 us -> 100 us
  local copies, waits for them, and re-layouts: 2.06 us -> 0.88 us
    pallas_call x1, Pallas kernels: 107 us -> 100 us  [pair_body(): pl.pallas_call(pair_kernel, out_shape=pltpu.VMEM((count, quarter), BF16),...]
    unnamed x1, local copies, waits for them, and re-layouts: 2.06 us -> 0.88 us
where the time goes in v1:
time: 101 us
  Pallas kernels  100 us (99%)
    pallas_call x1, Pallas kernels, pair_body(): pl.pallas_call(pair_kernel, out_shape=pltpu.VMEM((count, quarter), BF16),...  100 us

profile of v1, /device:TPU:0, one launch (start us, length us, event | category | flops | bytes accessed | tf_op | source)
XLA Modules:
  0.0 101.2 jit_solution(16560334703931816835)
XLA Ops:
  0.0 100.3 %shard_map.100 = bf16[768,512]{1,0:T(8,128)(2,1)S(1)} custom-call(bf16[768,512]{1,0:T(8,128)(2,1)} %tokens_hbm.1, f32[1,512]{1,0:T(1,128)} %bitcast.12, s32[2,768]{1,0:T(2,128)} %bitcast.10, f32[2,768]{1,0:T(2,128)} %bitcast.11, bf16[512,512]{1,0:T(8,128)(2,1)} %bitcast.7, bf16[512,512]{1,0:T(8,128)(2,1)} %bitcast.8, bf16[512,512]{1,0:T(8,128)(2,1)} %bitcast.9, ...), custom_call_target="tpu_custom_call" | custom-call | tf_op jit(solution)/shard_map/pallas_call | solution.py:671
  100.4 0.9 copy.12

commit v2 on v1

--- a/solution.py
+++ b/solution.py
@@ -92,7 +92,7 @@
 
 
 BF16, F32 = jnp.bfloat16, jnp.float32
-COPIES = 54
+COPIES = 61
 VMEM_LIMIT = 46 * 1024 * 1024
 
 
@@ -153,6 +153,7 @@
     cross_out,
     cross_in,
     branch_hidden,
+    branch_acc,
     code_col,
     factor_col,
     load_sem,
@@ -243,20 +244,34 @@
 
     slot_row = lax.broadcasted_iota(jnp.int32, (capacity, token_count), 0)
 
-    def choose_rows(s):
-        wanted = (slot_row + level[s] * capacity).astype(F32)
+    def choose_rows(s, where, target):
+        wanted = (slot_row + where * capacity).astype(F32)
         chosen[s] = jnp.where(wanted == code, 1.0, 0.0).astype(BF16)
-        rows = dot(chosen[s], scaled[0]).astype(BF16)
-        if s == 0:
-            slots[0] = rows
-        else:
-            slots_out[s] = rows
-
-    choose_rows(2)
+        target[s] = dot(chosen[s], scaled[0]).astype(BF16)
+
+    outer = (z == 0) | (z == GROUPS - 1)
+    near = jnp.where(outer, 1, 2)
+    choose_rows(near, jnp.where(outer, level[1], level[2]), slots_out)
 
     pl.semaphore_wait(barrier, len(peers))
 
     started = {}
+
+    def is_own(s):
+        return isinstance(s, int) and s == 0
+
+    def key_of(number):
+        return number if isinstance(number, int) else ("dynamic", len(started))
+
+    def wait_for(number, target):
+        pltpu.make_async_remote_copy(
+            src_ref=target,
+            dst_ref=target,
+            send_sem=send_sem.at[number],
+            recv_sem=recv_sem.at[number],
+            device_id=sibling,
+            device_id_type=pl.DeviceIdType.MESH,
+        ).wait_recv()
 
     def send(number, source, target, device):
         copy = pltpu.make_async_remote_copy(
@@ -268,7 +283,7 @@
             device_id_type=pl.DeviceIdType.MESH,
         )
         copy.start()
-        started[number] = copy
+        started[key_of(number)] = copy
 
     def send_if(condition, number, source, target, device):
         copy = pltpu.make_async_remote_copy(
@@ -359,13 +374,17 @@
     send(7, squares.at[0], squares.at[2], across)
     send(8, squares.at[0], squares.at[3], diagonal)
     send(6, squares.at[0], squares.at[1], sibling)
-    outer = (z == 0) | (z == GROUPS - 1)
     early = c == y
-    send_slots(2)
-    loads[5].wait()
-    loads[6].wait()
-    relay_start(1)
-    send_if(c != y, 10, scaled.at[0], scaled.at[2], across)
+    send_slots_if(outer, 1)
+    send_slots_if(~outer, 2)
+    part_rows = token_count // 2
+    first_rows, last_rows = pl.ds(0, part_rows), pl.ds(part_rows, part_rows)
+
+    def send_tokens(number, rows):
+        return number, scaled.at[0, rows], scaled.at[2, rows], across
+
+    send(*send_tokens(10, first_rows))
+    send_if(~early, *send_tokens(57, last_rows))
     for k in range(3):
         weight_copy(k, 0, pair_user).start()
 
@@ -374,6 +393,11 @@
         for k in range(3):
             weight_copy(k, 1, sibling).start()
 
+    choose_rows(3 - near, jnp.where(outer, level[2], level[1]), slots_out)
+    send_slots_if(outer, 2)
+    loads[5].wait()
+    loads[6].wait()
+    relay_start(1)
     send(9, scaled.at[0], scaled.at[1], sibling)
 
     def weight_arrived(k):
@@ -403,10 +427,9 @@
         rows = branch_all.at[y, level[m]]
         send(15 + m, rows, rows, pair)
 
-    choose_rows(0)
+    choose_rows(0, level[0], slots)
     send(26, slots.at[0], slots_s.at[0], sibling)
-    choose_rows(1)
-    choose_rows(3)
+    choose_rows(3, level[3], slots_out)
     pair_send(0)
 
     loads[3].wait()
@@ -426,14 +449,13 @@
     )
     weights_high = weights.astype(BF16)
     weights_low = (weights - weights_high.astype(F32)).astype(BF16)
-    for s in (2, 1, 3, 0):
+    for s in (2, 3, 1, 0):
         slot_weights = (dot_nt(weights_high, chosen[s]) + dot_nt(weights_low, chosen[s]))[:8]
         if s == 0:
             scale[0] = slot_weights
         else:
             scale_out[s] = slot_weights
             send_scale(s)
-    send_slots_if(outer, 1)
     send_slots_if(outer, 3)
 
     def project(s, start, weights):
@@ -445,36 +467,55 @@
     theirs = pl.multiple_of((1 - x) * half, half)
 
     def forward(s):
-        if s:
-            arrived(19 + s)
-            send(26 + s, slots.at[s], slots_s.at[s], sibling)
+        wait_for(19 + s, slots.at[s])
+        send(26 + s, slots.at[s], slots_s.at[s], sibling)
 
     sides = (slice(0, ff), slice(ff, 2 * ff))
 
     def stage_a(s):
-        arrived(26 + s)
+        wait_for(26 + s, slots_s.at[s])
         for side, weights in zip(sides, (gate_all, up_all)):
             part_out[s, :, side] = project(s, theirs, weights).astype(BF16)
         send(30 + s, part_out.at[s], part_in.at[s], across)
         for side, weights in zip(sides, (gate_all, up_all)):
             part_own[s, :, side] = project(s, mine, weights)
 
+    def stage_a_up_if(condition):
+        number, side = 50, sides[1]
+        copy = pltpu.make_async_remote_copy(
+            src_ref=part_out.at[0, :, side],
+            dst_ref=part_in.at[0, :, side],
+            send_sem=send_sem.at[number],
+            recv_sem=recv_sem.at[number],
+            device_id=across,
+            device_id_type=pl.DeviceIdType.MESH,
+        )
+        started[number] = copy
+
+        @pl.when(condition)
+        def _():
+            part_out[0, :, side] = project(0, theirs, up_all).astype(BF16)
+            copy.start()
+            part_own[0, :, side] = project(0, mine, up_all)
+
     def stage_a_side(s, k):
         if k == 0:
-            arrived(26 + s)
+            wait_for(26 + s, slots_s.at[s])
         side, weights = sides[k], (gate_all, up_all)[k]
         part_out[s, :, side] = project(s, theirs, weights).astype(BF16)
         number = 30 + s if k == 0 else 50 + s
         send(number, part_out.at[s, :, side], part_in.at[s, :, side], across)
         part_own[s, :, side] = project(s, mine, weights)
 
-    def stage_b(s):
-        if s:
-            arrived(22 + s)
+    def stage_b(s, sided=False):
+        if not is_own(s):
+            wait_for(22 + s, scale.at[s])
         scale_col[s] = jnp.transpose(scale[s])
-        arrived(30 + s)
-        if 50 + s in started:
-            arrived(50 + s)
+        if is_own(s) or sided:
+            wait_for(30 + s, part_in.at[s, :, sides[0]])
+            wait_for(50 + s, part_in.at[s, :, sides[1]])
+        else:
+            wait_for(30 + s, part_in.at[s])
         rescale = scale_col[s, pl.ds(mine, half), 2:3]
         gate_sum = (part_own[s, :, :ff] + part_in[s, :, :ff].astype(F32)) * rescale
         up_sum = (part_own[s, :, ff:] + part_in[s, :, ff:].astype(F32)) * rescale
@@ -483,7 +524,7 @@
         send(34 + s, kept, kept, across)
 
     def stage_c(s):
-        arrived(34 + s)
+        wait_for(34 + s, hidden.at[s, pl.ds(theirs, half), :])
         weight = jnp.where(c == 0, scale_col[s, :, 0:1], scale_col[s, :, 1:2])
         units = hidden[s]
         half_out[s] = (dot(units, down_all[1 - c]) * weight).astype(BF16)
@@ -491,43 +532,55 @@
         half_own[s] = dot(units, down_all[c]) * weight
 
     def stage_d(s):
-        arrived(38 + s)
+        wait_for(38 + s, half_in.at[s])
         both = (half_own[s] + half_in[s].astype(F32)).astype(BF16)
-        if s == 0:
+        if is_own(s):
             back[0] = both
         else:
             back_out[s] = both
-            send(41 + s, back_out.at[s], back.at[s], peer_of[s])
+            zone = level[s] if isinstance(s, int) else jnp.where(s == 1, level[1], level[3])
+            send(41 + s, back_out.at[s], back.at[s], at(zone, y, x, c))
 
     quarters = (tp, x * 2 + 1 - c, (1 - x) * 2 + c, (1 - x) * 2 + 1 - c)
 
-    def branch_first():
-        sums = jnp.zeros((token_count, block), F32)
-        for k, q in enumerate(quarters):
+    def branch_sum(members, first=False, last=False):
+        sums = jnp.zeros((token_count, block), F32) if first else branch_acc[...]
+        for m in members:
+            wait_for(15 + m, branch_all.at[1 - y, level[m]])
+            q = level[m]
+            k = (x + q // 2) % 2 * 2 + (c + q) % 2
             sums = sums + dot(scaled[k, :, :block], branch_all[0, q, 0])
             sums = sums + dot(scaled[k, :, block:], branch_all[1, q, 0])
-        branch_hidden[...] = silu(sums * factor_col[:, 0:1]).astype(BF16)
+        if last:
+            branch_hidden[...] = silu(sums * factor_col[:, 0:1]).astype(BF16)
+        else:
+            branch_acc[...] = sums
 
     def branch_part(q, side):
         return dot(branch_hidden[...], branch_all[side, q, 1])
 
+    left, right = slice(0, block), slice(block, 2 * block)
+
     def branch_fold():
-        for side in range(2):
-            columns = slice(side * block, (side + 1) * block)
+        for number, side, columns in ((54, 0, left), (55, 1, right)):
+            fold_out[1, :, columns] = branch_part(quarters[3], side).astype(BF16)
+            send(number, fold_out.at[1, :, columns], fold_in.at[1, :, columns], sibling)
+
+    def branch_fold_own():
+        for side, columns in ((0, left), (1, right)):
             fold_out[0, :, columns] = branch_part(quarters[1], side).astype(BF16)
-            fold_out[1, :, columns] = branch_part(quarters[3], side).astype(BF16)
-        send(45, fold_out, fold_in, sibling)
-
-    def branch_cross():
-        arrived(45)
-        for side in range(2):
-            columns = slice(side * block, (side + 1) * block)
-            cross_out[:, columns] = (
-                branch_part(quarters[2], side) + fold_in[1, :, columns].astype(F32)
-            ).astype(BF16)
-        send(46, cross_out, cross_in, across)
+        send(58, fold_out.at[0], fold_in.at[0], sibling)
+
+    def branch_cross(number, side, rows):
+        columns = (left, right)[side]
+        cross_out[rows, columns] = (
+            dot(branch_hidden[rows], branch_all[side, quarters[2], 1])
+            + fold_in[1, rows, columns].astype(F32)
+        ).astype(BF16)
+        send(number, cross_out.at[rows, columns], cross_in.at[rows, columns], across)
 
     def branch_own():
+        arrived(58)
         for side in range(2):
             columns = slice(side * block, (side + 1) * block)
             fold_own[:, columns] = branch_part(quarters[0], side) + fold_in[
@@ -538,61 +591,84 @@
 
     def restore(s):
         if s:
-            arrived(41 + s)
+            wait_for(41 + s, back.at[s])
         wanted = (slot_lane + level[s] * capacity).astype(F32)
         choose = jnp.where(wanted == code_col[:, 0:1], 1.0, 0.0).astype(BF16)
         return dot(choose, back[s])
 
+    first = jnp.where(outer, 3, 1)
+    last = 4 - first
     weight_arrived(0)
     stage_a_side(0, 0)
-    weight_arrived(1)
-    stage_a_side(0, 1)
-    send_if(early, 10, scaled.at[0], scaled.at[2], across)
+
+    @pl.when(early)
+    def _():
+        weight_arrived(1)
+
+    stage_a_up_if(early)
+    send_if(early & ~outer, *send_tokens(57, last_rows))
     forward(2)
-    send_slots_if(~outer, 3)
     send_slots_if(~outer, 1)
-    stage_a(2)
-    stage_b(0)
+    stage_a_side(2, 0)
+
+    @pl.when(~early)
+    def _():
+        weight_arrived(1)
+
+    stage_a_side(2, 1)
+    send_if(early & outer, *send_tokens(57, last_rows))
+    stage_a_up_if(~early)
     relay_arrived(1)
     relay_start(2)
+    send_slots_if(~outer, 3)
     pair_send(1)
-    arrived(10)
-    send(11, scaled.at[2], scaled.at[3], sibling)
-    forward(1)
-    stage_b(2)
+    stage_b(2, True)
+    stage_b(0)
+    forward(first)
+    stage_a_side(first, 0)
+    stage_a_side(first, 1)
     weight_arrived(2)
-    stage_c(0)
-    stage_d(0)
-    forward(3)
-    stage_a(3)
     stage_c(2)
-    stage_d(2)
     relay_arrived(2)
     relay_start(3)
     pair_send(2)
-    stage_a_side(1, 0)
-    stage_b(3)
-    stage_a_side(1, 1)
+    stage_c(0)
+    stage_d(0)
+    arrived(10)
+    arrived(57)
+    send(11, scaled.at[2], scaled.at[3], sibling)
+    forward(last)
+    stage_d(2)
+    stage_a_side(last, 0)
     relay_arrived(3)
     pair_send(3)
-    stage_c(3)
-    stage_d(3)
+    stage_b(first, True)
+    stage_a_side(last, 1)
     arrived(9)
     arrived(11)
-    for m in range(GROUPS):
-        arrived(15 + m)
-    branch_first()
+    branch_sum((0, 1, 2), first=True)
+    branch_sum((3,), last=True)
     branch_fold()
-    stage_b(1)
-    branch_cross()
+    arrived(54)
+    branch_cross(46, 0, slice(0, capacity))
+    stage_c(first)
+    stage_d(first)
+    stage_b(last, True)
+    branch_cross(59, 0, slice(capacity, token_count))
+    arrived(55)
+    branch_cross(60, 1, slice(0, token_count))
+    branch_fold_own()
+    stage_c(last)
+    stage_d(last)
     branch_own()
-    stage_c(1)
-    stage_d(1)
 
     half_own_sum = restore(0)
-    for s in (2, 3, 1):
-        half_own_sum = half_own_sum + restore(s)
+    half_own_sum = half_own_sum + restore(2)
+    half_own_sum = half_own_sum + restore(3)
+    half_own_sum = half_own_sum + restore(1)
     arrived(46)
+    arrived(59)
+    arrived(60)
     branch = fold_own[...] + cross_in[...].astype(F32)
     gate = 1.0 / (1.0 + jnp.exp(-branch_gate[...]))
     out[...] = (half_own_sum + gate * branch).astype(BF16)
@@ -662,6 +738,7 @@
         vmem((count, quarter), BF16),
         vmem((count, quarter), BF16),
         vmem((count, block), BF16),
+        vmem((count, block), F32),
         vmem((count, 8), F32),
         vmem((count, 8), F32),
         pltpu.SemaphoreType.DMA((10,)),

time: 101 us -> 94.5 us (0.936)
  Pallas kernels: 100 us -> 93.4 us
    pallas_call x1, Pallas kernels: 100 us -> 93.4 us  [pair_body(): pl.pallas_call(pair_kernel, out_shape=pltpu.VMEM((count, quarter), BF16),...]
where the time goes in v2:
time: 94.5 us; the launch traced here: 94.3 us
  Pallas kernels  93.4 us (99%)
    pallas_call x1, Pallas kernels, pair_body(): pl.pallas_call(pair_kernel, out_shape=pltpu.VMEM((count, quarter), BF16),...  93.4 us

profile of v2, /device:TPU:0, one launch (start us, length us, event | category | flops | bytes accessed | tf_op | source)
XLA Modules:
  0.0 94.3 jit_solution(16118744963815610533)
XLA Ops:
  0.0 93.4 %shard_map.100 = bf16[768,512]{1,0:T(8,128)(2,1)S(1)} custom-call(bf16[768,512]{1,0:T(8,128)(2,1)} %tokens_hbm.1, f32[1,512]{1,0:T(1,128)} %bitcast.12, s32[2,768]{1,0:T(2,128)} %bitcast.10, f32[2,768]{1,0:T(2,128)} %bitcast.11, bf16[512,512]{1,0:T(8,128)(2,1)} %bitcast.7, bf16[512,512]{1,0:T(8,128)(2,1)} %bitcast.8, bf16[512,512]{1,0:T(8,128)(2,1)} %bitcast.9, ...), custom_call_target="tpu_custom_call" | custom-call | tf_op jit(solution)/shard_map/pallas_call | solution.py:748
  93.4 0.9 copy.12

commit v3 on v2

--- a/solution.py
+++ b/solution.py
@@ -240,7 +240,7 @@
     high = exact.astype(BF16)
     low = (exact - high.astype(F32)).astype(BF16)
     ones = jnp.ones((16, quarter), BF16)
-    squares[0] = (dot_nt(ones, high) + dot_nt(ones, low))[:8]
+    squares[0] = (dot_nt(ones, high) + dot_nt(ones, low))[:1]
 
     slot_row = lax.broadcasted_iota(jnp.int32, (capacity, token_count), 0)
 
@@ -442,15 +442,15 @@
         arrived(number)
     total = squares[0] + squares[1] + squares[2] + squares[3]
     factor = lax.rsqrt(total / (4 * quarter) + epsilon)
-    factor_col[...] = jnp.transpose(factor)
+    factor_col[...] = jnp.transpose(jnp.broadcast_to(factor, (8, token_count)))
     code_col[...] = jnp.transpose(jnp.broadcast_to(code, (8, token_count)))
     weights = jnp.where(
-        rows16 == 0, for_even, jnp.where(rows16 == 1, for_odd, factor[0:1, :])
+        rows16 == 0, for_even, jnp.where(rows16 == 1, for_odd, factor)
     )
     weights_high = weights.astype(BF16)
     weights_low = (weights - weights_high.astype(F32)).astype(BF16)
     for s in (2, 3, 1, 0):
-        slot_weights = (dot_nt(weights_high, chosen[s]) + dot_nt(weights_low, chosen[s]))[:8]
+        slot_weights = (dot_nt(weights_high, chosen[s]) + dot_nt(weights_low, chosen[s]))[:4]
         if s == 0:
             scale[0] = slot_weights
         else:
@@ -510,7 +510,7 @@
     def stage_b(s, sided=False):
         if not is_own(s):
             wait_for(22 + s, scale.at[s])
-        scale_col[s] = jnp.transpose(scale[s])
+        scale_col[s] = jnp.transpose(jnp.concatenate([scale[s], scale[s]], axis=0))
         if is_own(s) or sided:
             wait_for(30 + s, part_in.at[s, :, sides[0]])
             wait_for(50 + s, part_in.at[s, :, sides[1]])
@@ -713,15 +713,15 @@
         vmem((2, quarter, ff), BF16),
         vmem((2, quarter, ff), BF16),
         vmem((2, ff, quarter), BF16),
-        vmem((4, 8, count), F32),
+        vmem((4, 1, count), F32),
         vmem((4, count, quarter), BF16),
         vmem((2, GROUPS, 2, block, block), BF16),
         vmem((GROUPS, cap, count), BF16),
         vmem(rows, BF16),
         vmem(rows, BF16),
         vmem(rows, BF16),
-        vmem((GROUPS, 8, cap), F32),
-        vmem((GROUPS, 8, cap), F32),
+        vmem((GROUPS, 4, cap), F32),
+        vmem((GROUPS, 4, cap), F32),
         vmem((GROUPS, cap, 8), F32),
         vmem((GROUPS, half, 2 * ff), BF16),
         vmem((GROUPS, half, 2 * ff), F32),

time: 94.5 us -> 93.9 us (level)
  no operation moved by 1% of the time
where the time goes in v3:
time: 93.9 us; the launch traced here: 93.8 us
  Pallas kernels  92.9 us (99%)
    pallas_call x1, Pallas kernels, pair_body(): pl.pallas_call(pair_kernel, out_shape=pltpu.VMEM((count, quarter), BF16),...  92.9 us

profile of v3, /device:TPU:0, one launch (start us, length us, event | category | flops | bytes accessed | tf_op | source)
XLA Modules:
  0.0 93.8 jit_solution(18081364211667024845)
XLA Ops:
  0.0 92.9 %shard_map.100 = bf16[768,512]{1,0:T(8,128)(2,1)S(1)} custom-call(bf16[768,512]{1,0:T(8,128)(2,1)} %tokens_hbm.1, f32[1,512]{1,0:T(1,128)} %bitcast.12, s32[2,768]{1,0:T(2,128)} %bitcast.10, f32[2,768]{1,0:T(2,128)} %bitcast.11, bf16[512,512]{1,0:T(8,128)(2,1)} %bitcast.7, bf16[512,512]{1,0:T(8,128)(2,1)} %bitcast.8, bf16[512,512]{1,0:T(8,128)(2,1)} %bitcast.9, ...), custom_call_target="tpu_custom_call" | custom-call | tf_op jit(solution)/shard_map/pallas_call | solution.py:748
  92.9 0.9 copy.12

commit v4 on v3

--- a/solution.py
+++ b/solution.py
@@ -571,13 +571,16 @@
             fold_out[0, :, columns] = branch_part(quarters[1], side).astype(BF16)
         send(58, fold_out.at[0], fold_in.at[0], sibling)
 
-    def branch_cross(number, side, rows):
+    def branch_cross(side, rows):
         columns = (left, right)[side]
         cross_out[rows, columns] = (
             dot(branch_hidden[rows], branch_all[side, quarters[2], 1])
             + fold_in[1, rows, columns].astype(F32)
         ).astype(BF16)
-        send(number, cross_out.at[rows, columns], cross_in.at[rows, columns], across)
+
+    def cross_piece(number, side, rows):
+        columns = (left, right)[side]
+        return number, cross_out.at[rows, columns], cross_in.at[rows, columns], across
 
     def branch_own():
         arrived(58)
@@ -650,15 +653,24 @@
     branch_sum((3,), last=True)
     branch_fold()
     arrived(54)
-    branch_cross(46, 0, slice(0, capacity))
+    branch_cross(0, slice(0, token_count))
+    pieces = (
+        cross_piece(46, 0, slice(0, capacity)),
+        cross_piece(59, 0, slice(capacity, token_count)),
+        cross_piece(60, 1, slice(0, token_count)),
+    )
+    send_if(early, *pieces[0])
     stage_c(first)
     stage_d(first)
     stage_b(last, True)
-    branch_cross(59, 0, slice(capacity, token_count))
+    send_if(~early, *pieces[0])
+    send(*pieces[1])
     arrived(55)
-    branch_cross(60, 1, slice(0, token_count))
+    branch_cross(1, slice(0, token_count))
+    send_if(early, *pieces[2])
     branch_fold_own()
     stage_c(last)
+    send_if(~early, *pieces[2])
     stage_d(last)
     branch_own()
 

time: 93.9 us -> 93.3 us (level); the launches traced: 93.8 us -> 91.8 us
  Pallas kernels: 92.9 us -> 90.9 us
    pallas_call x1, Pallas kernels: 92.9 us -> 90.9 us  [pair_body(): pl.pallas_call(pair_kernel, out_shape=pltpu.VMEM((count, quarter), BF16),...]
where the time goes in v4:
time: 93.3 us; the launch traced here: 91.8 us
  Pallas kernels  90.9 us (97%)
    pallas_call x1, Pallas kernels, pair_body(): pl.pallas_call(pair_kernel, out_shape=pltpu.VMEM((count, quarter), BF16),...  90.9 us

profile of v4, /device:TPU:0, one launch (start us, length us, event | category | flops | bytes accessed | tf_op | source)
XLA Modules:
  0.0 91.8 jit_solution(14589570701874948748)
XLA Ops:
  0.0 90.9 %shard_map.100 = bf16[768,512]{1,0:T(8,128)(2,1)S(1)} custom-call(bf16[768,512]{1,0:T(8,128)(2,1)} %tokens_hbm.1, f32[1,512]{1,0:T(1,128)} %bitcast.12, s32[2,768]{1,0:T(2,128)} %bitcast.10, f32[2,768]{1,0:T(2,128)} %bitcast.11, bf16[512,512]{1,0:T(8,128)(2,1)} %bitcast.7, bf16[512,512]{1,0:T(8,128)(2,1)} %bitcast.8, bf16[512,512]{1,0:T(8,128)(2,1)} %bitcast.9, ...), custom_call_target="tpu_custom_call" | custom-call | tf_op jit(solution)/shard_map/pallas_call | solution.py:760
  90.9 0.9 copy.12

commit v5 on v4

--- a/solution.py
+++ b/solution.py
@@ -92,7 +92,7 @@
 
 
 BF16, F32 = jnp.bfloat16, jnp.float32
-COPIES = 61
+COPIES = 62
 VMEM_LIMIT = 46 * 1024 * 1024
 
 
@@ -657,7 +657,8 @@
     pieces = (
         cross_piece(46, 0, slice(0, capacity)),
         cross_piece(59, 0, slice(capacity, token_count)),
-        cross_piece(60, 1, slice(0, token_count)),
+        cross_piece(60, 1, slice(0, capacity)),
+        cross_piece(61, 1, slice(capacity, token_count)),
     )
     send_if(early, *pieces[0])
     stage_c(first)
@@ -667,10 +668,11 @@
     send(*pieces[1])
     arrived(55)
     branch_cross(1, slice(0, token_count))
-    send_if(early, *pieces[2])
+    send(*pieces[2])
+    send_if(early, *pieces[3])
     branch_fold_own()
     stage_c(last)
-    send_if(~early, *pieces[2])
+    send_if(~early, *pieces[3])
     stage_d(last)
     branch_own()
 
@@ -681,6 +683,7 @@
     arrived(46)
     arrived(59)
     arrived(60)
+    arrived(61)
     branch = fold_own[...] + cross_in[...].astype(F32)
     gate = 1.0 / (1.0 + jnp.exp(-branch_gate[...]))
     out[...] = (half_own_sum + gate * branch).astype(BF16)

time: 93.3 us -> 93.3 us (level)
  no operation moved by 1% of the time
where the time goes in v5:
time: 93.3 us; the launch traced here: 91.8 us
  Pallas kernels  90.9 us (97%)
    pallas_call x1, Pallas kernels, pair_body(): pl.pallas_call(pair_kernel, out_shape=pltpu.VMEM((count, quarter), BF16),...  90.9 us

profile of v5, /device:TPU:0, one launch (start us, length us, event | category | flops | bytes accessed | tf_op | source)
XLA Modules:
  0.0 91.8 jit_solution(15114241511405087068)
XLA Ops:
  0.0 90.9 %shard_map.100 = bf16[768,512]{1,0:T(8,128)(2,1)S(1)} custom-call(bf16[768,512]{1,0:T(8,128)(2,1)} %tokens_hbm.1, f32[1,512]{1,0:T(1,128)} %bitcast.12, s32[2,768]{1,0:T(2,128)} %bitcast.10, f32[2,768]{1,0:T(2,128)} %bitcast.11, bf16[512,512]{1,0:T(8,128)(2,1)} %bitcast.7, bf16[512,512]{1,0:T(8,128)(2,1)} %bitcast.8, bf16[512,512]{1,0:T(8,128)(2,1)} %bitcast.9, ...), custom_call_target="tpu_custom_call" | custom-call | tf_op jit(solution)/shard_map/pallas_call | solution.py:763
  90.9 0.9 copy.12
